TPU v7x, 32 devices: a whole 2x2x4 slice. The times are simulated.
32 devices in a mesh: gr: 2 (over x), sp: 8 (over z, y), tp: 2 (over core).
Axes of the slice: x: 2, y: 2, z: 4, core: 2. Of those that a mesh axis runs over, the one named last changes fastest.
Arguments:
- context_input_tensor: bfloat16 [4, 8192, 2048], P(('gr', 'tp'), 'sp'), parts along dimension 0, may hold values from -8 to 8
- content_mapping_matrix: bfloat16 [2048, 1024], replicated, may hold values from -0.125 to 0.125
- address_mapping_matrix: bfloat16 [2048, 256], replicated, may hold values from -0.125 to 0.125
- increment_mapping_matrix: bfloat16 [2048, 16], replicated, may hold values from -0.125 to 0.125
- increment_speed_offset: float32 [16], P('sp'), may hold values from -1 to 0.5
- channel_fading_exponent: float32 [16], P('sp'), may hold values from -12 to -2
- extra_damping_spikes: float32 [4, 16, 8192], P(('gr', 'tp'), 'sp'), parts along dimension 0, may hold values from -3 to 0
- content_smoothing_coefficients: float32 [5, 16, 64], P(None, 'sp'), may hold values from -2.5 to 2.5
- address_smoothing_coefficients: float32 [5, 4, 64], replicated, may hold values from -2.5 to 2.5
- newest_lookup_matrix: bfloat16 [4, 4, 64], P(('gr', 'tp')), parts along dimension 0, may hold values from -6 to 6
- newest_output_switch: bfloat16 [4, 16, 64], P(('gr', 'tp'), 'sp'), parts along dimension 0, may hold values from -6 to 6
- cluster_scaling_coefficients: float32 [16, 64], P('sp'), may hold values from 0.1 to 1.9
Outputs:
- address_content_store: bfloat16 [4, 8192, 16, 128], P(('gr', 'tp'), None, 'sp'), parts along dimension 0
- earliest_switched_retrieval: bfloat16 [4, 16, 64], P(('gr', 'tp'), 'sp'), parts along dimension 0
There are 2 independent parts, one for each index of `gr`. A program takes and returns all parts, laid end to end along the dimension named above; an argument that names none is the same for every part. Nothing has to cross between parts.
All inputs are finite; a program needn't handle non-finite values.
Results may differ from a plain program's by a relative error of at most 0.009.
Values may be sent and summed in bfloat16 or wider, within the bound.
A program may use at most 128 MiB of HBM per device.

v0:
```python
import jax
import jax.numpy as jnp
from jax import lax
from jax.sharding import PartitionSpec as P

HEADS = 16
HEAD = 64
GROUPS = 4
STATE = 64


EPS = 1e-05


def swapped(value, axis, bit):
    mask = 2**bit
    pairs = [(source, source ^ mask) for source in range(lax.axis_size(axis))]
    return lax.ppermute(value, axis, pairs)


def centred(signal, kernel):
    margin = kernel.shape[0] // 2
    length = signal.shape[0]
    padded = jnp.pad(signal, ((margin, margin), (0, 0), (0, 0)))
    summed = kernel[0] * padded[0:length]
    for offset in range(1, kernel.shape[0]):
        summed = summed + kernel[offset] * padded[offset : offset + length]
    return summed


def on_device(
    context_input_tensor,
    content_mapping_matrix,
    address_mapping_matrix,
    increment_mapping_matrix,
    increment_speed_offset,
    channel_fading_exponent,
    extra_damping_spikes,
    content_smoothing_coefficients,
    address_smoothing_coefficients,
    newest_lookup_matrix,
    newest_output_switch,
    cluster_scaling_coefficients,
):
    prompt_token_rows = context_input_tensor[0]
    span_len = prompt_token_rows.shape[0]
    repeats = HEADS // GROUPS
    local_heads = increment_speed_offset.shape[0]
    group_devices = repeats // local_heads
    group_index = lax.axis_index("sp") * local_heads // repeats
    value_proj = (
        jnp.dot(prompt_token_rows, content_mapping_matrix, preferred_element_type=jnp.float32)
        .astype(jnp.bfloat16)
        .reshape(span_len, HEADS, HEAD)
    )
    key_proj = (
        jnp.dot(prompt_token_rows, address_mapping_matrix, preferred_element_type=jnp.float32)
        .astype(jnp.bfloat16)
        .reshape(span_len, GROUPS, STATE)
    )
    rate_raw = jnp.dot(
        prompt_token_rows, increment_mapping_matrix, preferred_element_type=jnp.float32
    ).astype(jnp.bfloat16)
    key_copies = jnp.repeat(key_proj, repeats, axis=1)
    value_seq, key_seq, rate_seq = (
        lax.all_to_all(value_proj, "sp", split_axis=1, concat_axis=0, tiled=True),
        lax.all_to_all(key_copies, "sp", split_axis=1, concat_axis=0, tiled=True),
        lax.all_to_all(rate_raw, "sp", split_axis=1, concat_axis=0, tiled=True),
    )
    key_group = key_seq[:, 0:1]
    seq_len = value_seq.shape[0]
    kernel_key = lax.dynamic_slice_in_dim(address_smoothing_coefficients, group_index, 1, 1)
    value_conv = jax.nn.silu(
        centred(value_seq.astype(jnp.float32), content_smoothing_coefficients)
    ).astype(jnp.bfloat16)
    key_conv = jax.nn.silu(centred(key_group.astype(jnp.float32), kernel_key)).astype(jnp.bfloat16)
    key_heads = jnp.broadcast_to(key_conv, (seq_len, local_heads, STATE))
    smoothed_increment_speed = jax.nn.softplus(
        rate_seq.astype(jnp.float32) + increment_speed_offset
    )
    exponent_increment_amount = (
        -jnp.exp(channel_fading_exponent) * smoothed_increment_speed + extra_damping_spikes[0].T
    )
    cumul = jnp.cumsum(exponent_increment_amount, axis=0)
    end_weight = jnp.exp(cumul[-1] - cumul)
    weighted = (
        value_conv.astype(jnp.float32) * (smoothed_increment_speed * end_weight)[:, :, None]
    ).astype(jnp.bfloat16)
    states = jnp.einsum("lhp,lhn->hpn", weighted, key_heads, preferred_element_type=jnp.float32)
    query_vector_row = lax.dynamic_slice_in_dim(newest_lookup_matrix[0], group_index, 1, 0).astype(
        jnp.float32
    )
    query_heads = jnp.broadcast_to(query_vector_row, (local_heads, STATE))
    raw_read = jnp.einsum("hpn,hn->hp", states, query_heads, precision=lax.Precision.HIGHEST)
    gated_read = raw_read * jax.nn.silu(newest_output_switch[0].astype(jnp.float32))
    group_sq = jnp.sum(gated_read * gated_read).reshape(1)
    for level in range(group_devices.bit_length() - 1):
        group_sq = group_sq + swapped(group_sq, "sp", level)
    scaled = (
        gated_read * lax.rsqrt(group_sq[0] / (repeats * HEAD) + EPS) * cluster_scaling_coefficients
    )
    kv_rows = jnp.concatenate([value_conv, key_heads], axis=-1)
    return (kv_rows[None], scaled.astype(jnp.bfloat16)[None])


def solution(mesh):
    placed = (
        P(("gr", "tp"), "sp", None),
        P(),
        P(),
        P(),
        P("sp"),
        P("sp"),
        P(("gr", "tp"), "sp", None),
        P(None, "sp", None),
        P(),
        P(("gr", "tp"), None, None),
        P(("gr", "tp"), "sp", None),
        P("sp", None),
    )
    return jax.shard_map(
        on_device,
        mesh=mesh,
        in_specs=placed,
        out_specs=(P(("gr", "tp"), None, "sp", None), P(("gr", "tp"), "sp", None)),
        check_vma=False,
    )
```

profile of v0, /device:TPU:0, one launch (start us, length us, event | category | flops | bytes accessed | tf_op | source)
XLA Modules:
  0.0 152.2 jit_solution(14708975432930272488)
XLA Ops:
  0.6 3.5 %fusion.15 = bf16[1024,16]{0,1:T(8,128)(2,1)S(1)} fusion(bf16[2048,16]{0,1:T(8,128)(2,1)} %param.15, bf16[1,1024,2048]{2,1,0:T(8,128)(2,1)} %param.12), kind=kOutput, calls=%fused_computation.18 | convolution fusion | flops 67125248 | bytes 4292608 | tf_op jit(solution)/shard_map/dot_general | solution.py:61
  4.1 0.7 all_to_all.35
  4.8 7.3 %all-to-all-start.2 = ((bf16[1024,8,2]{0,2,1:T(2,128)(2,1)}), bf16[1024,8,2]{0,2,1:T(2,128)(2,1)S(1)}, u32[]{:S(2)}, u32[]{:S(2)}) async-start(bf16[1024,8,2]{0,2,1:T(2,128)(2,1)} %all_to_all.35), calls=%async_computation.2 | async-start | bytes 65536 | tf_op jit(solution)/shard_map/all_to_all | solution.py:68
  12.1 3.5 %fusion.12 = bf16[1024,256]{0,1:T(8,128)(2,1)S(1)} fusion(bf16[2048,256]{1,0:T(8,128)(2,1)S(1)} %copy-done, bf16[1,1024,2048]{2,1,0:T(8,128)(2,1)} %param.12), kind=kOutput, calls=%fused_computation.17 | convolution fusion | flops 1074003968 | bytes 5767168 | tf_op jit(solution)/shard_map/dot_general | solution.py:57
  15.6 3.2 %all-to-all-done.2 = bf16[1024,8,2]{0,2,1:T(2,128)(2,1)S(1)} async-done(((bf16[1024,8,2]{0,2,1:T(2,128)(2,1)}), bf16[1024,8,2]{0,2,1:T(2,128)(2,1)S(1)}, u32[]{:S(2)}, u32[]{:S(2)}) %all-to-all-start.2) | async-done | bytes 32800 | tf_op jit(solution)/shard_map/all_to_all | solution.py:68
  18.8 1.6 %broadcast_in_dim.24 = bf16[1024,4,4,64]{0,3,2,1:T(8,128)(2,1)} broadcast(bf16[1024,4,64]{0,2,1:T(8,128)(2,1)S(1)} %bitcast.107), dimensions={0,1,3} | broadcast | bytes 2621440 | tf_op jit(solution)/shard_map/broadcast_in_dim | solution.py:64
  20.3 3.6 %all-to-all-start.1 = ((bf16[1024,16,64]{0,2,1:T(8,128)(2,1)}), bf16[1024,16,64]{0,2,1:T(8,128)(2,1)S(1)}, u32[]{:S(2)}, u32[]{:S(2)}) async-start(bf16[1024,16,64]{0,2,1:T(8,128)(2,1)} %bitcast.11), calls=%async_computation.1 | async-start | bytes 4194304 | tf_op jit(solution)/shard_map/all_to_all | solution.py:67
  24.0 0.8 fusion.28
  24.8 9.4 %fusion.9 = bf16[1024,1024]{0,1:T(8,128)(2,1)} fusion(bf16[2048,1024]{1,0:T(8,128)(2,1)} %param.13, bf16[1,1024,2048]{2,1,0:T(8,128)(2,1)} %param.12), kind=kOutput, calls=%fused_computation.16 | convolution fusion | flops 4296015872 | bytes 10485760 | tf_op jit(solution)/shard_map/dot_general | solution.py:52
  34.5 0.6 reduce-window.6
  35.7 35.2 %all-to-all-done.1 = bf16[1024,16,64]{0,2,1:T(8,128)(2,1)S(1)} async-done(((bf16[1024,16,64]{0,2,1:T(8,128)(2,1)}), bf16[1024,16,64]{0,2,1:T(8,128)(2,1)S(1)}, u32[]{:S(2)}, u32[]{:S(2)}) %all-to-all-start.1) | async-done | bytes 2097184 | tf_op jit(solution)/shard_map/all_to_all | solution.py:67
  71.0 1.3 copy-done.2
  72.3 3.8 %all-to-all-start = ((bf16[1024,16,64]{0,2,1:T(8,128)(2,1)}), bf16[1024,16,64]{0,2,1:T(8,128)(2,1)S(1)}, u32[]{:S(2)}, u32[]{:S(2)}) async-start(bf16[1024,16,64]{0,2,1:T(8,128)(2,1)} %bitcast.106), calls=%async_computation | async-start | bytes 4194304 | tf_op jit(solution)/shard_map/all_to_all | solution.py:66
  76.4 1.8 %copy.33 = bf16[8,2,8,8,1024]{4,3,0,2,1:T(8,128)(2,1)S(1)} copy(bf16[8,2,8,8,1024]{4,3,2,1,0:T(8,128)(2,1)} %bitcast.104) | data formatting | bytes 4194304 | tf_op jit(solution)/shard_map/all_to_all | solution.py:67
  78.2 1.5 slice_convert_fusion
  79.6 44.8 %all-to-all-done = bf16[1024,16,64]{0,2,1:T(8,128)(2,1)S(1)} async-done(((bf16[1024,16,64]{0,2,1:T(8,128)(2,1)}), bf16[1024,16,64]{0,2,1:T(8,128)(2,1)S(1)}, u32[]{:S(2)}, u32[]{:S(2)}) %all-to-all-start) | async-done | bytes 2097184 | tf_op jit(solution)/shard_map/all_to_all | solution.py:66
  125.2 1.3 copy-done.1
  126.4 2.4 %fusion.19 = bf16[8192,64]{0,1:T(8,128)(2,1)S(1)} fusion(f32[64]{0:T(128)S(1)} %get-tuple-element.14, f32[64]{0:T(128)S(1)} %get-tuple-element.11, f32[8192,1,64]{0,2,1:T(8,128)S(1)} %copy-done.1, f32[64]{0:T(128)S(1)} %get-tuple-element.12, f32[64]{0:T(128)S(1)} %get-tuple-element.13, f32[64]{0:T(128)S(1)} %get-tuple-element.10), kind=kLoop, calls=%fused_computation.21 | loop fusion | flops 7340032 | bytes 3147008 | tf_op jit(solution)/shard_map/broadcast_in_dim | solution.py:77
  128.9 4.7 %multiply_convert_fusion.1 = bf16[8192,2,64]{0,2,1:T(8,128)(2,1)S(1)} fusion(f32[8192,2,64]{0,2,1:T(8,128)S(1)} %bitcast.102, f32[2,64]{1,0:T(2,128)S(1)} %get-tuple-element.18, f32[2,64]{1,0:T(2,128)S(1)} %get-tuple-element.19, f32[2,64]{1,0:T(2,128)S(1)} %get-tuple-element.16, f32[2,64]{1,0:T(2,128)S(1)} %get-tuple-element.17, f32[2,64]{1,0:T(2,128)S(1)} %get-tuple-element.15), kind=kLoop, calls=%fused_computation.9 | loop fusion | flops 14680064 | bytes 6294016 | tf_op jit(solution)/shard_map/convert_element_type | solution.py:75
  133.6 0.7 fusion.8
  134.5 0.6 multiply_reduce_fusion
  135.2 1.4 collective-permute-start
  136.8 2.4 %maximum_bitcast_fusion = bf16[1,8192,2,128]{1,3,2,0:T(8,128)(2,1)} fusion(bf16[8192,2,64]{0,2,1:T(8,128)(2,1)S(1)} %broadcast_in_dim.26, bf16[8192,2,64]{0,2,1:T(8,128)(2,1)S(1)} %multiply_convert_fusion.1), kind=kLoop, calls=%fused_computation | loop fusion | flops 8388608 | bytes 8388608 | tf_op jit(solution)/shard_map/broadcast_in_dim | solution.py:103
  139.2 11.2 %copy.29 = bf16[1,8192,2,128]{3,2,1,0:T(2,128)(2,1)} copy(bf16[1,8192,2,128]{1,3,2,0:T(8,128)(2,1)} %maximum_bitcast_fusion) | data formatting | bytes 8388608
  (37 shorter events, 2.9 us)
Async XLA Ops:
  0.6 11.4 %copy-start = (bf16[2048,256]{1,0:T(8,128)(2,1)S(1)}, bf16[2048,256]{1,0:T(8,128)(2,1)}, u32[]{:S(2)}) copy-start(bf16[2048,256]{1,0:T(8,128)(2,1)} %param.14) | copy-start | bytes 3145732
  4.8 14.0 %all-to-all-start.2 = ((bf16[1024,8,2]{0,2,1:T(2,128)(2,1)}), bf16[1024,8,2]{0,2,1:T(2,128)(2,1)S(1)}, u32[]{:S(2)}, u32[]{:S(2)}) async-start(bf16[1024,8,2]{0,2,1:T(2,128)(2,1)} %all_to_all.35), calls=%async_computation.2 | async-start | bytes 65536 | tf_op jit(solution)/shard_map/all_to_all | solution.py:68
  15.6 8.4 %copy-start.8 = (bf16[1,4,64]{2,1,0:T(4,128)(2,1)S(1)}, bf16[1,4,64]{2,1,0:T(4,128)(2,1)}, u32[]{:S(2)}) copy-start(bf16[1,4,64]{2,1,0:T(4,128)(2,1)} %param.21) | copy-start | bytes 1540
  15.6 9.2 %copy-start.9 = (f32[2]{0:T(128)S(1)}, f32[2]{0:T(128)}, u32[]{:S(2)}) copy-start(f32[2]{0:T(128)} %param.17) | copy-start | bytes 28
  15.6 9.2 %copy-start.4 = (f32[5,2,64]{2,1,0:T(2,128)S(1)}, f32[5,2,64]{2,1,0:T(2,128)}, u32[]{:S(2)}) copy-start(f32[5,2,64]{2,1,0:T(2,128)} %param.19) | copy-start | bytes 7684
  20.3 50.6 %all-to-all-start.1 = ((bf16[1024,16,64]{0,2,1:T(8,128)(2,1)}), bf16[1024,16,64]{0,2,1:T(8,128)(2,1)S(1)}, u32[]{:S(2)}, u32[]{:S(2)}) async-start(bf16[1024,16,64]{0,2,1:T(8,128)(2,1)} %bitcast.11), calls=%async_computation.1 | async-start | bytes 4194304 | tf_op jit(solution)/shard_map/all_to_all | solution.py:67
  24.8 9.5 %copy-start.3 = (f32[1,2,8192]{2,1,0:T(2,128)S(1)}, f32[1,2,8192]{2,1,0:T(2,128)}, u32[]{:S(2)}) copy-start(f32[1,2,8192]{2,1,0:T(2,128)} %param.18) | copy-start | bytes 196612
  24.8 9.5 %copy-start.6 = (f32[2]{0:T(128)S(1)}, f32[2]{0:T(128)}, u32[]{:S(2)}) copy-start(f32[2]{0:T(128)} %param.16) | copy-start | bytes 28
  71.0 1.3 copy-start.2
  72.3 52.1 %all-to-all-start = ((bf16[1024,16,64]{0,2,1:T(8,128)(2,1)}), bf16[1024,16,64]{0,2,1:T(8,128)(2,1)S(1)}, u32[]{:S(2)}, u32[]{:S(2)}) async-start(bf16[1024,16,64]{0,2,1:T(8,128)(2,1)} %bitcast.106), calls=%async_computation | async-start | bytes 4194304 | tf_op jit(solution)/shard_map/all_to_all | solution.py:66
  124.8 1.6 %copy-start.1 = (f32[8192,1,64]{0,2,1:T(8,128)S(1)}, f32[8192,1,64]{0,2,1:T(8,128)}, u32[]{:S(2)}) copy-start(f32[8192,1,64]{0,2,1:T(8,128)} %slice_convert_fusion) | copy-start | bytes 6291460
  128.8 5.7 %copy-start.7 = (bf16[1,2,64]{2,1,0:T(2,128)(2,1)S(1)}, bf16[1,2,64]{2,1,0:T(2,128)(2,1)}, u32[]{:S(2)}) copy-start(bf16[1,2,64]{2,1,0:T(2,128)(2,1)} %param.22) | copy-start | bytes 772
  135.2 15.2 %collective-permute-start = (f32[1]{0:T(128)}, f32[1]{0:T(128)}, u32[]{:S(2)}, u32[]{:S(2)}) collective-permute-start(f32[1]{0:T(128)} %bitcast.32), channel_id=1, source_target_pairs={{0,2},{2,0},{4,6},{6,4},{8,10},{10,8},{12,14},{14,12},{1,3},{3,1},... | collective-permute-start | bytes 20 | tf_op jit(solution)/shard_map/ppermute | solution.py:18
  139.2 12.5 %copy-start.5 = (f32[2,64]{1,0:T(2,128)S(1)}, f32[2,64]{1,0:T(2,128)}, u32[]{:S(2)}) copy-start(f32[2,64]{1,0:T(2,128)} %param.23) | copy-start | bytes 1540
where the time goes:
time: 153 us; the launch traced here: 152 us
  waiting for transfers between devices  83.2 us (54%)
  local copies, waits for them, and re-layouts  19.6 us (13%)
  matrix products  17.2 us (11%)
  starting transfers between devices  16.1 us (11%)
  other arithmetic  13.9 us (9%)
  between operations  2.21 us (1%)
    all_to_all x1, waiting for transfers between devices, on_device(): lax.all_to_all(value_proj, 'sp', split_axis=1, concat_axis=0, tiled=True)  44.8 us
    all_to_all x1, waiting for transfers between devices, on_device(): lax.all_to_all(key_copies, 'sp', split_axis=1, concat_axis=0, tiled=True)  35.2 us
    unnamed x23, local copies, waits for them, and re-layouts  13.9 us
    dot_general x1, matrix products, on_device(): jnp.dot(prompt_token_rows, content_mapping_matrix, preferred_element_type...  9.4 us
    all_to_all x1, starting transfers between devices, on_device(): lax.all_to_all(rate_raw, 'sp', split_axis=1, concat_axis=0, tiled=True)  7.31 us
    convert_element_type x1, other arithmetic, on_device(): value_conv = jax.nn.silu(centred(value_seq.astype(jnp.float32), content_s...  4.75 us
    all_to_all x1, starting transfers between devices, on_device(): lax.all_to_all(value_proj, 'sp', split_axis=1, concat_axis=0, tiled=True)  3.78 us
    all_to_all x1, starting transfers between devices, on_device(): lax.all_to_all(key_copies, 'sp', split_axis=1, concat_axis=0, tiled=True)  3.6 us
  transfers between devices with their start and end apart: 4, of which 3 were waited for; matrix products, arithmetic and copies ran while one was open for 21% of the time, Pallas kernels for 0%

commit v1 on v0

--- a/solution.py
+++ b/solution.py
@@ -1,12 +1,18 @@
+import functools
+
 import jax
 import jax.numpy as jnp
 from jax import lax
+from jax.experimental import pallas as pl
+from jax.experimental.pallas import tpu as pltpu
 from jax.sharding import PartitionSpec as P
 
 HEADS = 16
 HEAD = 64
 GROUPS = 4
 STATE = 64
+KERNEL = 5
+GROUP_HEADS = HEADS // GROUPS
 
 
 EPS = 1e-05
@@ -103,6 +109,492 @@
     return (kv_rows[None], scaled.astype(jnp.bfloat16)[None])
 
 
+XLANES = 128
+MASKS = (2, 3, 1, 0)
+HALO = 16
+MESH = pl.DeviceIdType.MESH
+
+
+def flipped(index, mask):
+    total = 0
+    for bit in range(2):
+        digit = (index // 2**bit) % 2
+        total = total + 2**bit * ((1 - digit) if (mask >> bit) & 1 else digit)
+    return total
+
+
+def mixer_kernel(
+    n,
+    x_hbm,
+    wv_hbm,
+    wk_hbm,
+    wr_ref,
+    offset_ref,
+    fade_ref,
+    spikes_ref,
+    taps_ref,
+    key_taps_ref,
+    query_ref,
+    gate_ref,
+    gain_ref,
+    rows_out,
+    read_out,
+    x_ext,
+    wv,
+    wk,
+    proj,
+    taps_all,
+    key_send,
+    key_recv,
+    value_send,
+    value_recv,
+    rate_send,
+    rate_recv,
+    rate_rows,
+    spike_rows,
+    weights,
+    acc,
+    mixed,
+    packed,
+    square_send,
+    square_recv,
+    load_sem,
+    halo_send_sem,
+    halo_recv_sem,
+    taps_send_sem,
+    taps_recv_sem,
+    rate_send_sem,
+    rate_recv_sem,
+    key_send_sem,
+    key_recv_sem,
+    forward_sem,
+    value_send_sem,
+    value_recv_sem,
+    square_sem,
+    out_sem,
+):
+    span = x_hbm.shape[0]
+    half = span // 2
+    rows_ext = span + 2 * HALO
+    me = lax.axis_index("sp")
+    z, y = me // 2, me % 2
+    partner = 2 * z + 1 - y
+    chunk = 128
+    chunks = span // chunk
+
+    def remote(src, dst, send, recv, device):
+        return pltpu.make_async_remote_copy(
+            src_ref=src,
+            dst_ref=dst,
+            send_sem=send,
+            recv_sem=recv,
+            device_id={"sp": device},
+            device_id_type=MESH,
+        )
+
+    load_x = pltpu.make_async_copy(x_hbm, x_ext.at[pl.ds(HALO, span)], load_sem.at[0])
+    load_x.start()
+    load_k = pltpu.make_async_copy(wk_hbm, wk, load_sem.at[1])
+    load_k.start()
+    groups = [flipped(z, mask) for mask in MASKS]
+    load_v = []
+    for step, group in enumerate(groups):
+        columns = pl.ds(pl.multiple_of(group * 256, 256), 256)
+        load_v.append(
+            pltpu.make_async_copy(wv_hbm.at[:, columns], wv.at[step], load_sem.at[2 + step])
+        )
+        load_v[-1].start()
+
+    barrier = pltpu.get_barrier_semaphore()
+    for hop in range(1, n):
+        pl.semaphore_signal(
+            barrier, inc=1, device_id={"sp": (me + hop) % n}, device_id_type=MESH
+        )
+    own_taps = jnp.concatenate([taps_ref[:, 0, :], taps_ref[:, 1, :]], axis=1)
+    taps_all[me] = jnp.concatenate([own_taps, jnp.zeros((3, XLANES), jnp.float32)], axis=0)
+    pl.semaphore_wait(barrier, n - 1)
+
+    copies = []
+    after, before = (me + 1) % n, (me + n - 1) % n
+    halo_down = remote(
+        x_hbm.at[pl.ds(span - HALO, HALO)],
+        x_ext.at[pl.ds(0, HALO)],
+        halo_send_sem.at[0],
+        halo_recv_sem.at[0],
+        after,
+    )
+    halo_up = remote(
+        x_hbm.at[pl.ds(0, HALO)],
+        x_ext.at[pl.ds(span + HALO, HALO)],
+        halo_send_sem.at[1],
+        halo_recv_sem.at[1],
+        before,
+    )
+    halo_down.start()
+    halo_up.start()
+    for hop in range(1, n):
+        copy = remote(
+            taps_all.at[me],
+            taps_all.at[me],
+            taps_send_sem.at[hop],
+            taps_recv_sem.at[me],
+            (me + hop) % n,
+        )
+        copy.start()
+        copies.append(copy)
+
+    load_x.wait()
+    raw = jnp.dot(
+        x_ext[HALO : HALO + span, :], wr_ref[...], preferred_element_type=jnp.float32
+    )
+    raw = raw.astype(jnp.bfloat16).astype(jnp.float32).T
+    for device in range(n):
+        rate_send[device] = raw[2 * device : 2 * device + 2]
+    rate_recv[me] = rate_send[me]
+    for hop in range(1, n):
+        other = (me + hop) % n
+        copy = remote(
+            rate_send.at[other],
+            rate_recv.at[me],
+            rate_send_sem.at[hop],
+            rate_recv_sem.at[me],
+            other,
+        )
+        copy.start()
+        copies.append(copy)
+
+    halo_down.wait_recv()
+    halo_up.wait_recv()
+
+    @pl.when(me == 0)
+    def _():
+        x_ext[0:HALO, :] = jnp.zeros((HALO, x_ext.shape[1]), jnp.bfloat16)
+
+    @pl.when(me == n - 1)
+    def _():
+        x_ext[span + HALO :, :] = jnp.zeros((HALO, x_ext.shape[1]), jnp.bfloat16)
+
+    def project(weight):
+        piece = rows_ext // 2
+
+        @pl.loop(0, 2)
+        def _(index):
+            rows = pl.ds(pl.multiple_of(index * piece, 16), piece)
+            proj[rows, :] = (
+                jnp.dot(x_ext[rows, :], weight[...], preferred_element_type=jnp.float32)
+                .astype(jnp.bfloat16)
+                .astype(jnp.float32)
+            )
+
+    def smooth(index, taps):
+        window = proj[pl.ds(pl.multiple_of(index * chunk + 8, 8), chunk + 16), :]
+        summed = taps[0:1] * window[6 : 6 + chunk]
+        for tap in range(1, KERNEL):
+            summed = summed + taps[tap : tap + 1] * window[6 + tap : 6 + tap + chunk]
+        return summed * jax.nn.sigmoid(summed)
+
+    load_k.wait()
+    project(wk)
+    key_taps = jnp.concatenate([key_taps_ref[:, g, :] for g in range(GROUPS)], axis=1)
+    lane = lax.broadcasted_iota(jnp.int32, (chunk, XLANES), 1)
+
+    @pl.loop(0, chunks // 2)
+    def _(index):
+        first = smooth(index, key_taps)
+        second = smooth(index + chunks // 2, key_taps)
+        rows = pl.ds(pl.multiple_of(index * chunk, chunk), chunk)
+        for pair in range(2):
+            low = first[:, pair * XLANES : (pair + 1) * XLANES]
+            high = second[:, pair * XLANES : (pair + 1) * XLANES]
+            key_send[2 * pair, rows, :] = jnp.where(
+                lane < 64, low, pltpu.roll(high, 64, 1)
+            ).astype(jnp.bfloat16)
+            key_send[2 * pair + 1, rows, :] = jnp.where(
+                lane < 64, pltpu.roll(low, 64, 1), high
+            ).astype(jnp.bfloat16)
+
+    for step in range(3):
+        copy = remote(
+            key_send.at[groups[step]],
+            key_recv.at[me],
+            key_send_sem.at[step],
+            key_recv_sem.at[me],
+            2 * groups[step] + y,
+        )
+        copy.start()
+        copies.append(copy)
+    own_forward = remote(
+        key_send.at[z], key_recv.at[me], forward_sem.at[3], key_recv_sem.at[me], partner
+    )
+    own_forward.start()
+    copies.append(own_forward)
+    key_recv[me] = key_send[z]
+
+    for hop in range(1, n):
+        source = (me + hop) % n
+        remote(
+            taps_all.at[source],
+            taps_all.at[source],
+            taps_send_sem.at[hop],
+            taps_recv_sem.at[source],
+            source,
+        ).wait_recv()
+
+    for step, group in enumerate(groups):
+        load_v[step].wait()
+        project(wv.at[step])
+        taps = jnp.concatenate([taps_all[2 * group], taps_all[2 * group + 1]], axis=1)
+
+        @pl.loop(0, chunks)
+        def _(index):
+            value = smooth(index, taps).astype(jnp.bfloat16)
+            rows = pl.ds(pl.multiple_of(index * chunk, chunk), chunk)
+            value_send[step, 0, rows, :] = value[:, :XLANES]
+            value_send[step, 1, rows, :] = value[:, XLANES:]
+
+        for side in range(2):
+            if step < 3:
+                copy = remote(
+                    value_send.at[step, side],
+                    value_recv.at[me],
+                    value_send_sem.at[step, side],
+                    value_recv_sem.at[me],
+                    2 * group + side,
+                )
+                copy.start()
+                copies.append(copy)
+    last = remote(
+        value_send.at[3, 1 - y],
+        value_recv.at[me],
+        value_send_sem.at[3, 0],
+        value_recv_sem.at[me],
+        partner,
+    )
+    last.start()
+    copies.append(last)
+    value_recv[me] = value_send[3, y]
+
+    for hop in range(1, n):
+        source = (me + hop) % n
+        remote(
+            rate_send.at[source],
+            rate_recv.at[source],
+            rate_send_sem.at[hop],
+            rate_recv_sem.at[source],
+            source,
+        ).wait_recv()
+    for source in range(n):
+        rate_rows[2 * source : 2 * source + 2, :] = rate_recv[source]
+        spike_rows[2 * source : 2 * source + 2, :] = spikes_ref[
+            :, source * span : (source + 1) * span
+        ]
+    full = (2 * n, span)
+    odd = lax.broadcasted_iota(jnp.int32, full, 0) % 2 == 1
+    position = lax.broadcasted_iota(jnp.int32, full, 1)
+    shifted = rate_rows[...] + jnp.where(odd, offset_ref[1], offset_ref[0])
+    rate = jnp.maximum(shifted, 0.0) + jnp.log1p(jnp.exp(-jnp.abs(shifted)))
+    decay = jnp.exp(jnp.where(odd, fade_ref[1], fade_ref[0]))
+    later = spike_rows[...] - decay * rate
+    reach = 1
+    while reach < span:
+        later = later + jnp.where(
+            position < span - reach, pltpu.roll(later, span - reach, 1), 0.0
+        )
+        reach *= 2
+    blocks = jnp.broadcast_to(later[:, 0:1], (2 * n, XLANES))
+    block_row = lax.broadcasted_iota(jnp.int32, (2 * n, XLANES), 0)
+    reach = 2
+    while reach < 2 * n:
+        blocks = blocks + jnp.where(
+            block_row < 2 * n - reach, pltpu.roll(blocks, 2 * n - reach, 0), 0.0
+        )
+        reach *= 2
+    blocks = jnp.where(block_row < 2 * n - 2, pltpu.roll(blocks, 2 * n - 2, 0), 0.0)
+    later = jnp.where(position < span - 1, pltpu.roll(later, span - 1, 1), 0.0)
+    scaled = rate * jnp.exp(later + blocks[:, 0:1])
+    for source in range(n):
+        weights[source] = scaled[2 * source : 2 * source + 2]
+
+    queries = query_ref[...].astype(jnp.float32)
+    query_row = lax.broadcasted_iota(jnp.int32, queries.shape, 0)
+    query = jnp.sum(jnp.where(query_row == z, queries, 0.0), axis=0, keepdims=True)
+    blank = jnp.zeros((1, 64), jnp.float32)
+    asked = jnp.concatenate(
+        [
+            jnp.concatenate([query, blank], axis=1),
+            jnp.concatenate([blank, query], axis=1),
+            jnp.zeros((6, XLANES), jnp.float32),
+        ],
+        axis=0,
+    ).astype(jnp.bfloat16)
+    acc[...] = jnp.zeros_like(acc)
+
+    def take(source, slot):
+        scores = lax.dot_general(
+            asked,
+            key_recv[source],
+            (((1,), (1,)), ((), ())),
+            preferred_element_type=jnp.float32,
+        )
+        share = weights[source] * jnp.concatenate([scores[0:1], scores[1:2]], axis=1)
+        high = share.astype(jnp.bfloat16).astype(jnp.float32)
+        parts = jnp.concatenate(
+            [high, share - high, jnp.zeros((4, span), jnp.float32)], axis=0
+        ).astype(jnp.bfloat16)
+        acc[...] += jnp.dot(parts, value_recv[source], preferred_element_type=jnp.float32)
+
+        for part in range(2):
+
+            @pl.loop(0, chunks // 2)
+            def _(index):
+                at = pl.multiple_of(index * chunk, chunk)
+                value = value_recv[source, pl.ds(part * half + at, chunk), :].astype(jnp.float32)
+                key = key_recv[source, pl.ds(at, chunk), :].astype(jnp.float32)
+                if part == 0:
+                    key = pltpu.roll(key, 64, 1)
+                mixed[pl.ds(0, chunk, stride=2), :] = jnp.where(lane < 64, value, key)
+                mixed[pl.ds(1, chunk, stride=2), :] = jnp.where(
+                    lane < 64, pltpu.roll(value, 64, 1), key
+                )
+                packed[slot, pl.ds(2 * (part * half + at), 2 * chunk), :] = mixed[...].astype(
+                    jnp.bfloat16
+                )
+
+        out = pltpu.make_async_copy(
+            packed.at[slot],
+            rows_out.at[pl.ds(pl.multiple_of(source * 2 * span, 2 * span), 2 * span)],
+            out_sem.at[slot],
+        )
+        out.start()
+        return out
+
+    def key_wait(source):
+        remote(
+            key_recv.at[source],
+            key_recv.at[source],
+            forward_sem.at[0],
+            key_recv_sem.at[source],
+            partner,
+        ).wait_recv()
+
+    for step in range(3):
+        source = 2 * groups[step] + y
+        key_wait(source)
+        copy = remote(
+            key_recv.at[source],
+            key_recv.at[source],
+            forward_sem.at[step],
+            key_recv_sem.at[source],
+            partner,
+        )
+        copy.start()
+        copies.append(copy)
+
+    order = [(me, False, False), (partner, True, True)]
+    for step in range(3):
+        order.append((2 * groups[step] + y, False, True))
+        order.append((2 * groups[step] + 1 - y, True, True))
+    outs = []
+    for index, (source, wait_key, wait_value) in enumerate(order):
+        if wait_key:
+            key_wait(source)
+        if wait_value:
+            remote(
+                value_recv.at[source],
+                value_recv.at[source],
+                value_send_sem.at[0, 0],
+                value_recv_sem.at[source],
+                source,
+            ).wait_recv()
+        if index >= 2:
+            outs[index - 2].wait()
+        outs.append(take(source, index % 2))
+
+    total = acc[...]
+    first, second = total[0:1] + total[2:3], total[1:2] + total[3:4]
+    line = lax.broadcasted_iota(jnp.int32, (1, XLANES), 1)
+    raw_read = jnp.where(line < 64, first, second)
+    gate = gate_ref[...].astype(jnp.float32)
+    gate = jnp.concatenate([gate[0:1], gate[1:2]], axis=1)
+    gain = gain_ref[...]
+    gain = jnp.concatenate([gain[0:1], gain[1:2]], axis=1)
+    gated = raw_read * (gate * jax.nn.sigmoid(gate))
+    square = jnp.sum(gated * gated, axis=1, keepdims=True)
+    square_send[...] = jnp.broadcast_to(square, square_send.shape)
+    swap = remote(square_send, square_recv, square_sem.at[0], square_sem.at[1], partner)
+    swap.start()
+    swap.wait()
+    both = square + square_recv[0:1, 0:1]
+    result = gated * lax.rsqrt(both / (GROUP_HEADS * HEAD) + EPS) * gain
+    read_out[0:1, :] = result[:, :64]
+    read_out[1:2, :] = result[:, 64:]
+
+    outs[-2].wait()
+    outs[-1].wait()
+    halo_down.wait_send()
+    halo_up.wait_send()
+    for copy in copies:
+        copy.wait_send()
+
+
+def on_device_kernel(n, *arguments):
+    x, wv, wk, wr, offset, fade, spikes, taps, key_taps, query, gate, gain = arguments
+    span, model = x.shape[1:]
+    f32, bf16 = jnp.float32, jnp.bfloat16
+    vmem = pl.BlockSpec(memory_space=pltpu.VMEM)
+    smem = pl.BlockSpec(memory_space=pltpu.SMEM)
+    anywhere = pl.BlockSpec(memory_space=pl.ANY)
+    dma = pltpu.SemaphoreType.DMA
+    rows, read = pl.pallas_call(
+        functools.partial(mixer_kernel, n),
+        out_shape=(
+            jax.ShapeDtypeStruct((n * span * 2, 128), bf16),
+            jax.ShapeDtypeStruct((2, HEAD), f32),
+        ),
+        in_specs=[anywhere] * 3 + [vmem] + [smem] * 2 + [vmem] * 6,
+        out_specs=(anywhere, vmem),
+        scratch_shapes=[
+            pltpu.VMEM((span + 2 * HALO, model), bf16),
+            pltpu.VMEM((4, model, 256), bf16),
+            pltpu.VMEM((model, 256), bf16),
+            pltpu.VMEM((span + 2 * HALO, 256), f32),
+            pltpu.VMEM((n, 8, 128), f32),
+            pltpu.VMEM((GROUPS, span // 2, 128), bf16),
+            pltpu.VMEM((n, span // 2, 128), bf16),
+            pltpu.VMEM((4, 2, span, 128), bf16),
+            pltpu.VMEM((n, span, 128), bf16),
+            pltpu.VMEM((n, 2, span), f32),
+            pltpu.VMEM((n, 2, span), f32),
+            pltpu.VMEM((2 * n, span), f32),
+            pltpu.VMEM((2 * n, span), f32),
+            pltpu.VMEM((n, 2, span), f32),
+            pltpu.VMEM((8, 128), f32),
+            pltpu.VMEM((256, 128), f32),
+            pltpu.VMEM((2, 2 * span, 128), bf16),
+            pltpu.VMEM((8, 128), f32),
+            pltpu.VMEM((8, 128), f32),
+            dma((6,)),
+            dma((2,)),
+            dma((2,)),
+            dma((n,)),
+            dma((n,)),
+            dma((n,)),
+            dma((n,)),
+            dma((3,)),
+            dma((n,)),
+            dma((4,)),
+            dma((4, 2)),
+            dma((n,)),
+            dma((2,)),
+            dma((2,)),
+        ],
+        compiler_params=pltpu.CompilerParams(
+            collective_id=0, has_side_effects=True, vmem_limit_bytes=48 * 2**20
+        ),
+    )(x[0], wv, wk, wr, offset, fade, spikes[0], taps, key_taps, query[0], gate[0], gain)
+    return rows.reshape(1, n * span, 2, 2 * HEAD), read.astype(bf16)[None]
+
+
 def solution(mesh):
     placed = (
         P(("gr", "tp"), "sp", None),
@@ -118,8 +610,10 @@
         P(("gr", "tp"), "sp", None),
         P("sp", None),
     )
+    devices = mesh.shape["sp"]
+    pairs = HEADS == 2 * devices and GROUPS * 2 == devices
     return jax.shard_map(
-        on_device,
+        functools.partial(on_device_kernel, devices) if pairs else on_device,
         mesh=mesh,
         in_specs=placed,
         out_specs=(P(("gr", "tp"), None, "sp", None), P(("gr", "tp"), "sp", None)),

time: 153 us -> 88.5 us (0.58)
  the two profiles are of different devices: /device:TPU:0 before, /device:TPU:18 now
where the time goes in v1:
time: 88.5 us; the launch traced here: 88.1 us
  Pallas kernels  77.1 us (87%)
  local copies, waits for them, and re-layouts  9.9 us (11%)
    pallas_call x1, Pallas kernels, on_device_kernel(): pl.pallas_call(functools.partial(mixer_kernel, n), out_shape=(jax.ShapeDt...  77.1 us
    unnamed x20, local copies, waits for them, and re-layouts  9.9 us

profile of v1, /device:TPU:18, one launch (start us, length us, event | category | flops | bytes accessed | tf_op | source)
XLA Modules:
  0.0 88.1 jit_solution(10880887652989124284)
XLA Ops:
  0.6 1.1 %copy.14.wr_ref = bf16[2048,16]{1,0:T(8,128)(2,1)S(1)} copy(bf16[2048,16]{0,1:T(8,128)(2,1)} %param.15) | data formatting | bytes 131072 | tf_op args[3]
  1.7 0.0 copy-start
  1.8 1.2 %copy-done = bf16[2048,256]{1,0:T(8,128)(2,1)S(1)} copy-done((bf16[2048,256]{1,0:T(8,128)(2,1)S(1)}, bf16[2048,256]{1,0:T(8,128)(2,1)}, u32[]{:S(2)}) %copy-start) | copy-done | bytes 1048600
  3.0 0.0 copy-start.1
  3.0 0.8 copy-done.1
  3.8 0.0 copy-start.2
  3.8 0.7 copy-done.2
  4.5 0.0 copy-start.3
  4.5 0.7 copy-done.3
  5.2 0.0 copy-start.4
  5.2 0.7 copy-done.4
  5.9 0.0 copy-start.5
  5.9 0.7 copy-done.5
  6.6 0.0 copy-start.6
  6.6 0.7 copy-done.6
  7.2 0.0 copy-start.7
  7.2 0.7 copy-done.7
  7.9 0.0 copy-start.8
  7.9 0.7 copy-done.8
  8.5 77.1 %shard_map.131 = (bf16[16384,128]{1,0:T(8,128)(2,1)S(1)}, f32[2,64]{1,0:T(2,128)S(1)}) custom-call(bf16[1024,2048]{1,0:T(8,128)(2,1)} %bitcast.11, bf16[2048,1024]{1,0:T(8,128)(2,1)} %wv_hbm.1, bf16[2048,256]{1,0:T(8,128)(2,1)S(1)} %copy-done, bf16[2048,16]{1,0:T(8,128)(2,1)S(1)} %copy.14.wr_ref, f32[2]{0:T(128)S(1)} %copy-done.6, f32[2]{0:T(128)S(1)} %copy-done.7, ...), custom_call_target="tpu_custom_call" | custom-call | tf_op jit(solution)/shard_map/pallas_call | solution.py:548
  85.6 0.5 convert_bitcast_fusion
  86.1 2.0 %copy.16 = bf16[1,8192,2,128]{3,2,1,0:T(2,128)(2,1)} copy(bf16[1,8192,2,128]{3,2,1,0:T(2,128)(2,1)S(1)} %bitcast.7) | data formatting | bytes 8388608
Async XLA Ops:
  1.7 1.2 %copy-start = (bf16[2048,256]{1,0:T(8,128)(2,1)S(1)}, bf16[2048,256]{1,0:T(8,128)(2,1)}, u32[]{:S(2)}) copy-start(bf16[2048,256]{1,0:T(8,128)(2,1)} %wk_hbm.1) | copy-start | bytes 3145732
  3.0 0.8 copy-start.1
  3.8 0.7 copy-start.2
  4.5 0.7 copy-start.3
  5.2 0.7 copy-start.4
  5.9 0.7 copy-start.5
  6.6 0.7 copy-start.6
  7.2 0.7 copy-start.7
  7.9 0.7 copy-start.8

commit v2 on v1

--- a/solution.py
+++ b/solution.py
@@ -110,16 +110,21 @@
 
 
 XLANES = 128
-MASKS = (2, 3, 1, 0)
 HALO = 16
+INNER = (2, 0, 1, 3)
+OUTER = (1, 0, 2, 3)
+INNER_KEYS = (3, 2, 1)
+OUTER_KEYS = (1, 2, 3)
 MESH = pl.DeviceIdType.MESH
 
 
-def flipped(index, mask):
+def flipped(index, inner, outer):
+    low, high = index % 2, (index // 2) % 2
+    inside = low + high - 2 * low * high
     total = 0
-    for bit in range(2):
-        digit = (index // 2**bit) % 2
-        total = total + 2**bit * ((1 - digit) if (mask >> bit) & 1 else digit)
+    for bit, digit in enumerate((low, high)):
+        flip = inside * ((inner >> bit) & 1) + (1 - inside) * ((outer >> bit) & 1)
+        total = total + 2**bit * (digit + flip - 2 * digit * flip)
     return total
 
 
@@ -128,6 +133,17 @@
     x_hbm,
     wv_hbm,
     wk_hbm,
+    wr_hbm,
+    offset_hbm,
+    fade_hbm,
+    spikes_hbm,
+    taps_hbm,
+    key_taps_hbm,
+    query_hbm,
+    gate_hbm,
+    gain_hbm,
+    rows_out,
+    read_out,
     wr_ref,
     offset_ref,
     fade_ref,
@@ -137,8 +153,7 @@
     query_ref,
     gate_ref,
     gain_ref,
-    rows_out,
-    read_out,
+    small_sem,
     x_ext,
     wv,
     wk,
@@ -192,11 +207,37 @@
             device_id_type=MESH,
         )
 
-    load_x = pltpu.make_async_copy(x_hbm, x_ext.at[pl.ds(HALO, span)], load_sem.at[0])
-    load_x.start()
+    small = []
+    for index, (source, target) in enumerate(
+        (
+            (taps_hbm, taps_ref),
+            (key_taps_hbm, key_taps_ref),
+            (wr_hbm, wr_ref),
+            (offset_hbm, offset_ref),
+            (fade_hbm, fade_ref),
+            (spikes_hbm, spikes_ref),
+            (query_hbm, query_ref),
+            (gate_hbm, gate_ref),
+            (gain_hbm, gain_ref),
+        )
+    ):
+        small.append(pltpu.make_async_copy(source, target, small_sem.at[index]))
+    small[0].start()
+    load_x = [
+        pltpu.make_async_copy(
+            x_hbm.at[pl.ds(part * half, half)],
+            x_ext.at[pl.ds(HALO + part * half, half)],
+            load_sem.at[6 * part],
+        )
+        for part in range(2)
+    ]
     load_k = pltpu.make_async_copy(wk_hbm, wk, load_sem.at[1])
     load_k.start()
-    groups = [flipped(z, mask) for mask in MASKS]
+    load_x[0].start()
+    load_x[1].start()
+    groups = [flipped(z, inner, outer) for inner, outer in zip(INNER, OUTER)]
+    key_groups = [flipped(z, inner, outer) for inner, outer in zip(INNER_KEYS, OUTER_KEYS)]
+    own_step = INNER.index(0)
     load_v = []
     for step, group in enumerate(groups):
         columns = pl.ds(pl.multiple_of(group * 256, 256), 256)
@@ -204,12 +245,15 @@
             pltpu.make_async_copy(wv_hbm.at[:, columns], wv.at[step], load_sem.at[2 + step])
         )
         load_v[-1].start()
+    for copy in small[1:]:
+        copy.start()
 
     barrier = pltpu.get_barrier_semaphore()
     for hop in range(1, n):
         pl.semaphore_signal(
             barrier, inc=1, device_id={"sp": (me + hop) % n}, device_id_type=MESH
         )
+    small[0].wait()
     own_taps = jnp.concatenate([taps_ref[:, 0, :], taps_ref[:, 1, :]], axis=1)
     taps_all[me] = jnp.concatenate([own_taps, jnp.zeros((3, XLANES), jnp.float32)], axis=0)
     pl.semaphore_wait(barrier, n - 1)
@@ -243,48 +287,19 @@
         copy.start()
         copies.append(copy)
 
-    load_x.wait()
-    raw = jnp.dot(
-        x_ext[HALO : HALO + span, :], wr_ref[...], preferred_element_type=jnp.float32
-    )
-    raw = raw.astype(jnp.bfloat16).astype(jnp.float32).T
-    for device in range(n):
-        rate_send[device] = raw[2 * device : 2 * device + 2]
-    rate_recv[me] = rate_send[me]
-    for hop in range(1, n):
-        other = (me + hop) % n
-        copy = remote(
-            rate_send.at[other],
-            rate_recv.at[me],
-            rate_send_sem.at[hop],
-            rate_recv_sem.at[me],
-            other,
-        )
-        copy.start()
-        copies.append(copy)
-
-    halo_down.wait_recv()
-    halo_up.wait_recv()
-
-    @pl.when(me == 0)
-    def _():
-        x_ext[0:HALO, :] = jnp.zeros((HALO, x_ext.shape[1]), jnp.bfloat16)
-
-    @pl.when(me == n - 1)
-    def _():
-        x_ext[span + HALO :, :] = jnp.zeros((HALO, x_ext.shape[1]), jnp.bfloat16)
+    piece = rows_ext // 2
+
+    def project_rows(weight, rows):
+        proj[rows, :] = (
+            jnp.dot(x_ext[rows, :], weight[...], preferred_element_type=jnp.float32)
+            .astype(jnp.bfloat16)
+            .astype(jnp.float32)
+        )
 
     def project(weight):
-        piece = rows_ext // 2
-
         @pl.loop(0, 2)
         def _(index):
-            rows = pl.ds(pl.multiple_of(index * piece, 16), piece)
-            proj[rows, :] = (
-                jnp.dot(x_ext[rows, :], weight[...], preferred_element_type=jnp.float32)
-                .astype(jnp.bfloat16)
-                .astype(jnp.float32)
-            )
+            project_rows(weight, pl.ds(pl.multiple_of(index * piece, 16), piece))
 
     def smooth(index, taps):
         window = proj[pl.ds(pl.multiple_of(index * chunk + 8, 8), chunk + 16), :]
@@ -294,7 +309,23 @@
         return summed * jax.nn.sigmoid(summed)
 
     load_k.wait()
-    project(wk)
+    load_x[0].wait()
+    halo_down.wait_recv()
+
+    @pl.when(me == 0)
+    def _():
+        x_ext[0:HALO, :] = jnp.zeros((HALO, x_ext.shape[1]), jnp.bfloat16)
+
+    project_rows(wk, pl.ds(0, piece))
+    load_x[1].wait()
+    halo_up.wait_recv()
+
+    @pl.when(me == n - 1)
+    def _():
+        x_ext[span + HALO :, :] = jnp.zeros((HALO, x_ext.shape[1]), jnp.bfloat16)
+
+    project_rows(wk, pl.ds(piece, piece))
+    small[1].wait()
     key_taps = jnp.concatenate([key_taps_ref[:, g, :] for g in range(GROUPS)], axis=1)
     lane = lax.broadcasted_iota(jnp.int32, (chunk, XLANES), 1)
 
@@ -315,11 +346,11 @@
 
     for step in range(3):
         copy = remote(
-            key_send.at[groups[step]],
+            key_send.at[key_groups[step]],
             key_recv.at[me],
             key_send_sem.at[step],
             key_recv_sem.at[me],
-            2 * groups[step] + y,
+            2 * key_groups[step] + y,
         )
         copy.start()
         copies.append(copy)
@@ -340,6 +371,53 @@
             source,
         ).wait_recv()
 
+    def send_rates():
+        small[2].wait()
+        raw = lax.dot_general(
+            wr_ref[...],
+            x_ext[HALO : HALO + span, :],
+            (((1,), (1,)), ((), ())),
+            preferred_element_type=jnp.float32,
+        )
+        raw = raw.astype(jnp.bfloat16).astype(jnp.float32)
+        for device in range(n):
+            rate_send[device] = raw[2 * device : 2 * device + 2]
+        rate_recv[me] = rate_send[me]
+        for hop in range(1, n):
+            other = (me + hop) % n
+            copy = remote(
+                rate_send.at[other],
+                rate_recv.at[me],
+                rate_send_sem.at[hop],
+                rate_recv_sem.at[me],
+                other,
+            )
+            copy.start()
+            copies.append(copy)
+
+    def key_wait(source):
+        remote(
+            key_recv.at[source],
+            key_recv.at[source],
+            forward_sem.at[0],
+            key_recv_sem.at[source],
+            partner,
+        ).wait_recv()
+
+    def forward_keys():
+        for step in range(3):
+            source = 2 * key_groups[step] + y
+            key_wait(source)
+            copy = remote(
+                key_recv.at[source],
+                key_recv.at[source],
+                forward_sem.at[step],
+                key_recv_sem.at[source],
+                partner,
+            )
+            copy.start()
+            copies.append(copy)
+
     for step, group in enumerate(groups):
         load_v[step].wait()
         project(wv.at[step])
@@ -352,8 +430,19 @@
             value_send[step, 0, rows, :] = value[:, :XLANES]
             value_send[step, 1, rows, :] = value[:, XLANES:]
 
-        for side in range(2):
-            if step < 3:
+        if step == own_step:
+            copy = remote(
+                value_send.at[step, 1 - y],
+                value_recv.at[me],
+                value_send_sem.at[step, 0],
+                value_recv_sem.at[me],
+                partner,
+            )
+            copy.start()
+            copies.append(copy)
+            value_recv[me] = value_send[step, y]
+        else:
+            for side in range(2):
                 copy = remote(
                     value_send.at[step, side],
                     value_recv.at[me],
@@ -363,17 +452,12 @@
                 )
                 copy.start()
                 copies.append(copy)
-    last = remote(
-        value_send.at[3, 1 - y],
-        value_recv.at[me],
-        value_send_sem.at[3, 0],
-        value_recv_sem.at[me],
-        partner,
-    )
-    last.start()
-    copies.append(last)
-    value_recv[me] = value_send[3, y]
-
+        if step == 0:
+            send_rates()
+        if step == 2:
+            forward_keys()
+    for wanted in small[3:]:
+        wanted.wait()
     for hop in range(1, n):
         source = (me + hop) % n
         remote(
@@ -391,9 +475,9 @@
     full = (2 * n, span)
     odd = lax.broadcasted_iota(jnp.int32, full, 0) % 2 == 1
     position = lax.broadcasted_iota(jnp.int32, full, 1)
-    shifted = rate_rows[...] + jnp.where(odd, offset_ref[1], offset_ref[0])
+    shifted = rate_rows[...] + jnp.where(odd, offset_ref[0:1, 1:2], offset_ref[0:1, 0:1])
     rate = jnp.maximum(shifted, 0.0) + jnp.log1p(jnp.exp(-jnp.abs(shifted)))
-    decay = jnp.exp(jnp.where(odd, fade_ref[1], fade_ref[0]))
+    decay = jnp.exp(jnp.where(odd, fade_ref[0:1, 1:2], fade_ref[0:1, 0:1]))
     later = spike_rows[...] - decay * rate
     reach = 1
     while reach < span:
@@ -429,7 +513,7 @@
     ).astype(jnp.bfloat16)
     acc[...] = jnp.zeros_like(acc)
 
-    def take(source, slot):
+    def read(source):
         scores = lax.dot_general(
             asked,
             key_recv[source],
@@ -443,6 +527,7 @@
         ).astype(jnp.bfloat16)
         acc[...] += jnp.dot(parts, value_recv[source], preferred_element_type=jnp.float32)
 
+    def assemble(source, slot):
         for part in range(2):
 
             @pl.loop(0, chunks // 2)
@@ -468,30 +553,8 @@
         out.start()
         return out
 
-    def key_wait(source):
-        remote(
-            key_recv.at[source],
-            key_recv.at[source],
-            forward_sem.at[0],
-            key_recv_sem.at[source],
-            partner,
-        ).wait_recv()
-
-    for step in range(3):
-        source = 2 * groups[step] + y
-        key_wait(source)
-        copy = remote(
-            key_recv.at[source],
-            key_recv.at[source],
-            forward_sem.at[step],
-            key_recv_sem.at[source],
-            partner,
-        )
-        copy.start()
-        copies.append(copy)
-
     order = [(me, False, False), (partner, True, True)]
-    for step in range(3):
+    for step in (2, 0, 3):
         order.append((2 * groups[step] + y, False, True))
         order.append((2 * groups[step] + 1 - y, True, True))
     outs = []
@@ -506,9 +569,11 @@
                 value_recv_sem.at[source],
                 source,
             ).wait_recv()
-        if index >= 2:
-            outs[index - 2].wait()
-        outs.append(take(source, index % 2))
+        read(source)
+        if index < n - 1:
+            if index >= 2:
+                outs[index - 2].wait()
+            outs.append(assemble(source, index % 2))
 
     total = acc[...]
     first, second = total[0:1] + total[2:3], total[1:2] + total[3:4]
@@ -523,6 +588,8 @@
     square_send[...] = jnp.broadcast_to(square, square_send.shape)
     swap = remote(square_send, square_recv, square_sem.at[0], square_sem.at[1], partner)
     swap.start()
+    outs[n - 3].wait()
+    outs.append(assemble(order[-1][0], (n - 1) % 2))
     swap.wait()
     both = square + square_recv[0:1, 0:1]
     result = gated * lax.rsqrt(both / (GROUP_HEADS * HEAD) + EPS) * gain
@@ -542,8 +609,19 @@
     span, model = x.shape[1:]
     f32, bf16 = jnp.float32, jnp.bfloat16
     vmem = pl.BlockSpec(memory_space=pltpu.VMEM)
-    smem = pl.BlockSpec(memory_space=pltpu.SMEM)
     anywhere = pl.BlockSpec(memory_space=pl.ANY)
+    stored = pl.BlockSpec(memory_space=pltpu.HBM)
+    small = (
+        wr.T,
+        offset.reshape(1, 2),
+        fade.reshape(1, 2),
+        spikes[0],
+        taps,
+        key_taps,
+        query[0],
+        gate[0],
+        gain,
+    )
     dma = pltpu.SemaphoreType.DMA
     rows, read = pl.pallas_call(
         functools.partial(mixer_kernel, n),
@@ -551,9 +629,11 @@
             jax.ShapeDtypeStruct((n * span * 2, 128), bf16),
             jax.ShapeDtypeStruct((2, HEAD), f32),
         ),
-        in_specs=[anywhere] * 3 + [vmem] + [smem] * 2 + [vmem] * 6,
+        in_specs=[stored] * (3 + len(small)),
         out_specs=(anywhere, vmem),
-        scratch_shapes=[
+        scratch_shapes=[pltpu.VMEM(value.shape, value.dtype) for value in small]
+        + [
+            dma((len(small),)),
             pltpu.VMEM((span + 2 * HALO, model), bf16),
             pltpu.VMEM((4, model, 256), bf16),
             pltpu.VMEM((model, 256), bf16),
@@ -573,7 +653,7 @@
             pltpu.VMEM((2, 2 * span, 128), bf16),
             pltpu.VMEM((8, 128), f32),
             pltpu.VMEM((8, 128), f32),
-            dma((6,)),
+            dma((7,)),
             dma((2,)),
             dma((2,)),
             dma((n,)),
@@ -589,9 +669,9 @@
             dma((2,)),
         ],
         compiler_params=pltpu.CompilerParams(
-            collective_id=0, has_side_effects=True, vmem_limit_bytes=48 * 2**20
+            collective_id=0, has_side_effects=True, vmem_limit_bytes=61000000
         ),
-    )(x[0], wv, wk, wr, offset, fade, spikes[0], taps, key_taps, query[0], gate[0], gain)
+    )(x[0], wv, wk, *small)
     return rows.reshape(1, n * span, 2, 2 * HEAD), read.astype(bf16)[None]
 
 

time: 88.5 us -> 86.3 us (0.975)
  local copies, waits for them, and re-layouts: 9.9 us -> 7.7 us
    unnamed x20 -> x1, local copies, waits for them, and re-layouts: 9.9 us -> 7.7 us
where the time goes in v2:
time: 86.3 us; the launch traced here: 85.9 us
  Pallas kernels  76.4 us (89%)
  local copies, waits for them, and re-layouts  7.7 us (9%)
  other arithmetic  1.15 us (1%)
    pallas_call x1, Pallas kernels, on_device_kernel(): pl.pallas_call(functools.partial(mixer_kernel, n), out_shape=(jax.ShapeDt...  76.4 us
    unnamed x1, local copies, waits for them, and re-layouts  7.7 us

profile of v2, /device:TPU:18, one launch (start us, length us, event | category | flops | bytes accessed | tf_op | source)
XLA Modules:
  0.0 85.9 jit_solution(15557377948377872426)
XLA Ops:
  0.6 76.4 %shard_map.131 = (bf16[16384,128]{1,0:T(8,128)(2,1)}, f32[2,64]{1,0:T(2,128)}) custom-call(bf16[1024,2048]{1,0:T(8,128)(2,1)} %bitcast.10, bf16[2048,1024]{1,0:T(8,128)(2,1)} %wv_hbm.1, bf16[2048,256]{1,0:T(8,128)(2,1)} %wk_hbm.1, bf16[16,2048]{1,0:T(8,128)(2,1)} %bitcast.12, f32[1,2]{1,0:T(1,128)} %bitcast.15, f32[1,2]{1,0:T(1,128)} %bitcast.16, ...), custom_call_target="tpu_custom_call" | custom-call | tf_op jit(solution)/shard_map/pallas_call | solution.py:626
  77.0 1.1 %convert_bitcast_fusion = bf16[1,2,64]{2,1,0:T(2,128)(2,1)} fusion(f32[2,64]{1,0:T(2,128)} %get-tuple-element.5), kind=kLoop, calls=%fused_computation | loop fusion | flops 128 | bytes 768 | tf_op jit(solution)/shard_map/broadcast_in_dim | solution.py:675
  78.2 7.7 %copy.15 = bf16[1,8192,2,128]{3,2,1,0:T(2,128)(2,1)} copy(bf16[1,8192,2,128]{3,2,1,0:T(2,128)(2,1)} %bitcast.11) | data formatting | bytes 8388608

commit v3 on v2

--- a/solution.py
+++ b/solution.py
@@ -113,6 +113,8 @@
 HALO = 16
 INNER = (2, 0, 1, 3)
 OUTER = (1, 0, 2, 3)
+ARRIVALS = (2, 0, 3)
+FORWARD_STEP = 2
 INNER_KEYS = (3, 2, 1)
 OUTER_KEYS = (1, 2, 3)
 MESH = pl.DeviceIdType.MESH
@@ -170,7 +172,6 @@
     weights,
     acc,
     mixed,
-    packed,
     square_send,
     square_recv,
     load_sem,
@@ -186,7 +187,6 @@
     value_send_sem,
     value_recv_sem,
     square_sem,
-    out_sem,
 ):
     span = x_hbm.shape[0]
     half = span // 2
@@ -444,17 +444,17 @@
         else:
             for side in range(2):
                 copy = remote(
-                    value_send.at[step, side],
+                    value_send.at[step, (y + side) % 2],
                     value_recv.at[me],
                     value_send_sem.at[step, side],
                     value_recv_sem.at[me],
-                    2 * group + side,
+                    2 * group + (y + side) % 2,
                 )
                 copy.start()
                 copies.append(copy)
         if step == 0:
             send_rates()
-        if step == 2:
+        if step == FORWARD_STEP:
             forward_keys()
     for wanted in small[3:]:
         wanted.wait()
@@ -527,7 +527,7 @@
         ).astype(jnp.bfloat16)
         acc[...] += jnp.dot(parts, value_recv[source], preferred_element_type=jnp.float32)
 
-    def assemble(source, slot):
+    def assemble(source):
         for part in range(2):
 
             @pl.loop(0, chunks // 2)
@@ -541,23 +541,13 @@
                 mixed[pl.ds(1, chunk, stride=2), :] = jnp.where(
                     lane < 64, pltpu.roll(value, 64, 1), key
                 )
-                packed[slot, pl.ds(2 * (part * half + at), 2 * chunk), :] = mixed[...].astype(
-                    jnp.bfloat16
-                )
-
-        out = pltpu.make_async_copy(
-            packed.at[slot],
-            rows_out.at[pl.ds(pl.multiple_of(source * 2 * span, 2 * span), 2 * span)],
-            out_sem.at[slot],
-        )
-        out.start()
-        return out
+                line = pl.multiple_of(2 * (source * span + part * half + at), 2 * chunk)
+                rows_out[pl.ds(line, 2 * chunk), :] = mixed[...].astype(jnp.bfloat16)
 
     order = [(me, False, False), (partner, True, True)]
-    for step in (2, 0, 3):
+    for step in ARRIVALS:
         order.append((2 * groups[step] + y, False, True))
         order.append((2 * groups[step] + 1 - y, True, True))
-    outs = []
     for index, (source, wait_key, wait_value) in enumerate(order):
         if wait_key:
             key_wait(source)
@@ -571,9 +561,7 @@
             ).wait_recv()
         read(source)
         if index < n - 1:
-            if index >= 2:
-                outs[index - 2].wait()
-            outs.append(assemble(source, index % 2))
+            assemble(source)
 
     total = acc[...]
     first, second = total[0:1] + total[2:3], total[1:2] + total[3:4]
@@ -588,16 +576,13 @@
     square_send[...] = jnp.broadcast_to(square, square_send.shape)
     swap = remote(square_send, square_recv, square_sem.at[0], square_sem.at[1], partner)
     swap.start()
-    outs[n - 3].wait()
-    outs.append(assemble(order[-1][0], (n - 1) % 2))
+    assemble(order[-1][0])
     swap.wait()
     both = square + square_recv[0:1, 0:1]
     result = gated * lax.rsqrt(both / (GROUP_HEADS * HEAD) + EPS) * gain
     read_out[0:1, :] = result[:, :64]
     read_out[1:2, :] = result[:, 64:]
 
-    outs[-2].wait()
-    outs[-1].wait()
     halo_down.wait_send()
     halo_up.wait_send()
     for copy in copies:
@@ -609,7 +594,6 @@
     span, model = x.shape[1:]
     f32, bf16 = jnp.float32, jnp.bfloat16
     vmem = pl.BlockSpec(memory_space=pltpu.VMEM)
-    anywhere = pl.BlockSpec(memory_space=pl.ANY)
     stored = pl.BlockSpec(memory_space=pltpu.HBM)
     small = (
         wr.T,
@@ -626,11 +610,11 @@
     rows, read = pl.pallas_call(
         functools.partial(mixer_kernel, n),
         out_shape=(
-            jax.ShapeDtypeStruct((n * span * 2, 128), bf16),
-            jax.ShapeDtypeStruct((2, HEAD), f32),
+            pltpu.VMEM((n * span * 2, 128), bf16),
+            pltpu.VMEM((2, HEAD), f32),
         ),
         in_specs=[stored] * (3 + len(small)),
-        out_specs=(anywhere, vmem),
+        out_specs=(vmem, vmem),
         scratch_shapes=[pltpu.VMEM(value.shape, value.dtype) for value in small]
         + [
             dma((len(small),)),
@@ -650,7 +634,6 @@
             pltpu.VMEM((n, 2, span), f32),
             pltpu.VMEM((8, 128), f32),
             pltpu.VMEM((256, 128), f32),
-            pltpu.VMEM((2, 2 * span, 128), bf16),
             pltpu.VMEM((8, 128), f32),
             pltpu.VMEM((8, 128), f32),
             dma((7,)),
@@ -666,10 +649,9 @@
             dma((4, 2)),
             dma((n,)),
             dma((2,)),
-            dma((2,)),
         ],
         compiler_params=pltpu.CompilerParams(
-            collective_id=0, has_side_effects=True, vmem_limit_bytes=61000000
+            collective_id=0, has_side_effects=True, vmem_limit_bytes=56 * 2**20
         ),
     )(x[0], wv, wk, *small)
     return rows.reshape(1, n * span, 2, 2 * HEAD), read.astype(bf16)[None]

time: 86.3 us -> 78.2 us (0.906)
  local copies, waits for them, and re-layouts: 7.7 us -> 2.02 us
  Pallas kernels: 76.4 us -> 74 us
    unnamed x1, local copies, waits for them, and re-layouts: 7.7 us -> 2.02 us
    pallas_call x1, Pallas kernels: 76.4 us -> 74 us  [on_device_kernel(): pl.pallas_call(functools.partial(mixer_kernel, n), out_shape=(pltpu.VMEM(...]
where the time goes in v3:
time: 78.2 us; the launch traced here: 77.2 us
  Pallas kernels  74 us (95%)
  local copies, waits for them, and re-layouts  2.02 us (3%)
    pallas_call x1, Pallas kernels, on_device_kernel(): pl.pallas_call(functools.partial(mixer_kernel, n), out_shape=(pltpu.VMEM(...  74 us
    unnamed x1, local copies, waits for them, and re-layouts  2.02 us

profile of v3, /device:TPU:18, one launch (start us, length us, event | category | flops | bytes accessed | tf_op | source)
XLA Modules:
  0.0 77.2 jit_solution(441447238529589048)
XLA Ops:
  0.6 74.0 %shard_map.131 = (bf16[16384,128]{1,0:T(8,128)(2,1)S(1)}, f32[2,64]{1,0:T(2,128)S(1)}) custom-call(bf16[1024,2048]{1,0:T(8,128)(2,1)} %bitcast.11, bf16[2048,1024]{1,0:T(8,128)(2,1)} %wv_hbm.1, bf16[2048,256]{1,0:T(8,128)(2,1)} %wk_hbm.1, bf16[16,2048]{1,0:T(8,128)(2,1)} %bitcast.12, f32[1,2]{1,0:T(1,128)} %bitcast.15, f32[1,2]{1,0:T(1,128)} %bitcast.16, ...), custom_call_target="tpu_custom_call" | custom-call | tf_op jit(solution)/shard_map/pallas_call | solution.py:610
  74.6 2.0 %copy.15 = bf16[1,8192,2,128]{3,2,1,0:T(2,128)(2,1)} copy(bf16[1,8192,2,128]{3,2,1,0:T(2,128)(2,1)S(1)} %bitcast.10) | data formatting | bytes 8388608
  76.6 0.5 convert_bitcast_fusion
